TPU v7x, 32 devices: a whole 2x2x4 slice. The times are simulated.
32 devices in a mesh: ep: 8 (over z, core), tp: 4 (over y, x).
Axes of the slice: x: 2, y: 2, z: 4, core: 2. Of those that a mesh axis runs over, the one named last changes fastest.
Arguments:
- queries: bfloat16 [2048, 2048], P('ep', 'tp'), may hold values from -6 to 6
- keys: bfloat16 [2048, 2048], P('ep', 'tp'), may hold values from -6 to 6
- values: bfloat16 [2048, 2048], P('ep', 'tp'), may hold values from -6 to 6
- gates: bfloat16 [2048, 2048], P('ep', 'tp'), may hold values from -6 to 6
- log_decay: float32 [2048, 16], P('ep', 'tp'), may hold values from -2 to 0
- out_weight: bfloat16 [2048, 2048], P(None, 'tp'), may hold values from -0.125 to 0.125
- moe_rows: bfloat16 [2048, 2048], P('ep'), may hold values from -140 to 140
- moe_gain: bfloat16 [2048], replicated, may hold values from 0.099609375 to 1.8984375
- routes: int32 [2048, 2], P('ep'), may hold values from 0 to 7, as said below
- route_weights: float32 [2048, 2], P('ep'), may hold values from 0.1 to 1
- gate_proj: bfloat16 [8, 2048, 4096], P('ep', None, 'tp'), may hold values from -0.125 to 0.125
- up_proj: bfloat16 [8, 2048, 4096], P('ep', None, 'tp'), may hold values from -0.125 to 0.125
- down_proj: bfloat16 [8, 4096, 2048], P('ep', None, 'tp'), may hold values from -0.09375 to 0.09375
Outputs:
- mixer_out: bfloat16 [2048, 2048], P('ep', 'tp')
- moe_out: bfloat16 [2048, 2048], P('ep', 'tp')
Inputs may be any that keep to these rules, and one draw needn't show every extreme that they name: `routes`: each row names two different experts of one group of 8 consecutive experts; in each aligned block of 256 rows every expert is named by exactly 64 rows.
All inputs are finite; a program needn't handle non-finite values.
Results may differ from a plain program's by a relative error of at most 0.011.
Values may be sent and summed in bfloat16 or wider, within the bound.
A program may use at most 64 MiB of HBM per device.

v0:
```python
import jax
import jax.numpy as jnp
from jax import lax
from jax.sharding import PartitionSpec as P

BLOCK = 128


def carried_in(value, axis, join, neutral):
    count, mine = (lax.axis_size(axis), lax.axis_index(axis))
    pieces = jax.tree.map(lambda part: lax.all_gather(part, axis), value)
    total = jax.tree.map(
        lambda part, zero: jnp.full_like(part, 0) + jnp.asarray(zero, part.dtype), value, neutral
    )

    def turn(position, total):
        longer = join(total, jax.tree.map(lambda part: part[position], pieces))
        return jax.tree.map(lambda new, old: jnp.where(position < mine, new, old), longer, total)

    return lax.fori_loop(0, count - 1, turn, total)


def rotate(source, positions, heads_here, factor):
    row_count, feat_width = source.shape
    head_dim = feat_width // heads_here
    half_dim = head_dim // 2
    values_f = source.astype(jnp.float32).reshape(row_count, heads_here, head_dim)
    inverse = 10000.0 ** (-jnp.arange(half_dim, dtype=jnp.float32) / half_dim)
    angles = positions[:, None] * inverse[None, :]
    cosine = jnp.cos(angles)[:, None, :]
    sine_part = jnp.sin(angles)[:, None, :]
    first_half = values_f[..., :half_dim]
    second_half = values_f[..., half_dim:]
    turned = jnp.concatenate(
        [
            first_half * cosine - second_half * sine_part,
            first_half * sine_part + second_half * cosine,
        ],
        axis=-1,
    )
    return (turned * factor).astype(jnp.bfloat16).reshape(row_count, feat_width)


def chain_states(earlier, later):
    return (earlier[0] * later[0], later[0][:, None, None] * earlier[1] + later[1])


def retention_half(queries, keys, values, gates, log_decay, out_weight):
    row_count, feat_width = queries.shape
    heads_here = log_decay.shape[1]
    head_dim = feat_width // heads_here
    block_count = row_count // BLOCK
    positions = (lax.axis_index("ep") * row_count + jnp.arange(row_count, dtype=jnp.int32)).astype(
        jnp.float32
    )
    rot_q = rotate(queries, positions, heads_here, 1.0)
    rot_k = rotate(keys, positions, heads_here, head_dim ** (-0.5))
    block_shape = (block_count, BLOCK, heads_here, head_dim)
    q_blocks = rot_q.reshape(block_shape)
    k_blocks = rot_k.reshape(block_shape)
    v_blocks = values.reshape(block_shape)
    cumulative = jnp.cumsum(log_decay.reshape(block_count, BLOCK, heads_here), axis=1)
    across = jnp.swapaxes(cumulative, 1, 2)
    spread = across[..., :, None] - across[..., None, :]
    causal = jnp.arange(BLOCK)[:, None] >= jnp.arange(BLOCK)[None, :]
    weights = jnp.where(causal, jnp.exp(jnp.where(causal, spread, 0.0)), 0.0)
    scores = jnp.einsum("nihd,njhd->nhij", q_blocks, k_blocks, preferred_element_type=jnp.float32)
    rounded = (scores * weights).astype(jnp.bfloat16)
    inside = jnp.einsum("nhij,njhd->nihd", rounded, v_blocks, preferred_element_type=jnp.float32)
    ending = cumulative[:, -1, :]
    k_scaled = k_blocks.astype(jnp.float32) * jnp.exp(ending[:, None, :] - cumulative)[..., None]
    updates = jnp.einsum(
        "njhd,njhe->nhde", k_scaled, v_blocks.astype(jnp.float32), precision=lax.Precision.HIGHEST
    )

    def advance(carry_state, member):
        return (jnp.exp(member[0])[:, None, None] * carry_state + member[1], carry_state)

    zero_state = jnp.zeros((heads_here, head_dim, head_dim), jnp.float32)
    local_end, before = lax.scan(advance, zero_state, (ending, updates))
    device_decay = jnp.exp(jnp.sum(ending, axis=0))
    incoming = carried_in(
        (device_decay, local_end), "ep", chain_states, (jnp.ones_like(device_decay), zero_state)
    )
    leading = jnp.cumsum(ending, axis=0) - ending
    entering = before + jnp.exp(leading)[:, :, None, None] * incoming[1][None]
    carried = (
        jnp.einsum(
            "nihd,nhde->nihe",
            q_blocks.astype(jnp.float32),
            entering,
            precision=lax.Precision.HIGHEST,
        )
        * jnp.exp(cumulative)[..., None]
    )
    retained = (inside + carried).reshape(row_count, heads_here, head_dim)
    gate_f = gates.astype(jnp.float32).reshape(row_count, heads_here, head_dim)
    scaled = retained * lax.rsqrt(jnp.mean(retained * retained, axis=-1, keepdims=True) + 1e-05)
    head_out = (scaled * jax.nn.silu(gate_f)).astype(jnp.bfloat16).reshape(row_count, feat_width)
    projected = jnp.dot(
        lax.all_gather(head_out, "tp", axis=1, tiled=True),
        out_weight,
        preferred_element_type=jnp.float32,
    )
    return projected.astype(jnp.bfloat16)


def expert_half(moe_rows, moe_gain, routes, route_weights, gate_proj, up_proj, down_proj):
    row_count, feat_width = moe_rows.shape
    experts = lax.axis_size("ep")
    capacity = 2 * row_count // experts
    as_float = moe_rows.astype(jnp.float32)
    normed = (
        as_float
        * lax.rsqrt(jnp.mean(as_float * as_float, axis=-1, keepdims=True) + 1e-06)
        * moe_gain.astype(jnp.float32)
    ).astype(jnp.bfloat16)
    flat_ids = routes.reshape(-1)
    onehot = (flat_ids[:, None] == jnp.arange(experts, dtype=jnp.int32)[None, :]).astype(jnp.int32)
    slot_rank = jnp.sum((jnp.cumsum(onehot, axis=0) - onehot) * onehot, axis=1)
    target = flat_ids * capacity + slot_rank
    source_row = (
        jnp.zeros((experts * capacity,), jnp.int32)
        .at[target]
        .set(jnp.arange(2 * row_count, dtype=jnp.int32) // 2)
    )
    outgoing = normed[source_row].reshape(experts, capacity, feat_width)
    w_gate = gate_proj[0]
    w_up = up_proj[0]
    w_down = down_proj[0]
    arrived_rows = lax.all_to_all(outgoing, "ep", split_axis=0, concat_axis=0, tiled=True)
    gate_part = jnp.einsum("scd,df->scf", arrived_rows, w_gate, preferred_element_type=jnp.float32)
    up_part = jnp.einsum("scd,df->scf", arrived_rows, w_up, preferred_element_type=jnp.float32)
    hidden = (jax.nn.silu(gate_part) * up_part).astype(jnp.bfloat16)
    expert_out = jnp.einsum(
        "scf,fd->scd",
        lax.all_gather(hidden, "tp", axis=2, tiled=True),
        w_down,
        preferred_element_type=jnp.float32,
    ).astype(jnp.bfloat16)
    returned = lax.all_to_all(expert_out, "ep", split_axis=0, concat_axis=0, tiled=True)
    picked = returned.reshape(experts * capacity, -1)[target].reshape(row_count, 2, -1)
    return jnp.sum(picked.astype(jnp.float32) * route_weights[:, :, None], axis=1).astype(
        jnp.bfloat16
    )


def on_device(
    queries,
    keys,
    values,
    gates,
    log_decay,
    out_weight,
    moe_rows,
    moe_gain,
    routes,
    route_weights,
    gate_proj,
    up_proj,
    down_proj,
):
    mixer_out = retention_half(queries, keys, values, gates, log_decay, out_weight)
    moe_out = expert_half(moe_rows, moe_gain, routes, route_weights, gate_proj, up_proj, down_proj)
    return (mixer_out, moe_out)


def solution(mesh):
    placed = (
        P("ep", "tp"),
        P("ep", "tp"),
        P("ep", "tp"),
        P("ep", "tp"),
        P("ep", "tp"),
        P(None, "tp"),
        P("ep", None),
        P(),
        P("ep", None),
        P("ep", None),
        P("ep", None, "tp"),
        P("ep", None, "tp"),
        P("ep", None, "tp"),
    )
    return jax.shard_map(
        on_device,
        mesh=mesh,
        in_specs=placed,
        out_specs=(P("ep", "tp"), P("ep", "tp")),
        check_vma=False,
    )
```

profile of v0, /device:TPU:17, one launch (start us, length us, event | category | flops | bytes accessed | tf_op | source)
XLA Modules:
  0.0 197.7 jit_solution(13536535929649242897)
XLA Ops:
  10.9 2.4 %scatter_custom_fusion = s32[512]{0:T(512)S(1)} fusion(s32[512]{0:T(512)S(1)} %bitcast.110, s32[512]{0:T(512)S(1)} %add_select_fusion, s32[]{:T(128)} %copy.125), kind=kCustom, calls=%fused_computation.90 | custom fusion | bytes 2052 | tf_op jit(solution)/shard_map/scatter | solution.py:125
  15.6 1.5 fusion.11
  17.2 3.3 %gather_fusion = bf16[512,2048]{1,0:T(8,128)(2,1)} fusion(bf16[256,2048]{1,0:T(8,128)(2,1)S(1)} %fusion.11, s32[1024]{0:T(1024)S(1)} %pad_clamp_fusion.1), kind=kCustom, calls=%fused_computation | custom fusion | bytes 4196352 | tf_op jit(solution)/shard_map/gather | solution.py:127
  20.5 5.6 %all-to-all-start = ((bf16[8,64,2048]{2,1,0:T(8,128)(2,1)}), bf16[8,64,2048]{2,1,0:T(8,128)(2,1)}, u32[]{:S(2)}, u32[]{:S(2)}) async-start(bf16[8,64,2048]{2,1,0:T(8,128)(2,1)} %bitcast.100), calls=%async_computation | async-start | bytes 4194304 | tf_op jit(solution)/shard_map/all_to_all | solution.py:131
  30.0 1.8 concatenate.21
  36.5 1.7 reshape.218
  39.2 1.7 fusion.27
  40.9 1.7 while.29
  43.4 44.8 %all-to-all-done = bf16[8,64,2048]{2,1,0:T(8,128)(2,1)} async-done(((bf16[8,64,2048]{2,1,0:T(8,128)(2,1)}), bf16[8,64,2048]{2,1,0:T(8,128)(2,1)}, u32[]{:S(2)}, u32[]{:S(2)}) %all-to-all-start) | async-done | bytes 2097184 | tf_op jit(solution)/shard_map/all_to_all | solution.py:131
  88.1 5.3 %fusion.7 = f32[8,64,1024]{2,1,0:T(8,128)S(1)} fusion(bf16[8,64,2048]{2,1,0:T(8,128)(2,1)} %all-to-all-done, bf16[1,2048,1024]{2,1,0:T(8,128)(2,1)} %param.27), kind=kOutput, calls=%fused_computation.15 | convolution fusion | flops 2147483648 | bytes 8388608 | tf_op jit(solution)/shard_map/scd,df->scf/dot_general | solution.py:132
  93.5 5.2 %multiply_convert_fusion = bf16[8,64,1024]{2,1,0:T(8,128)(2,1)} fusion(f32[8,64,1024]{2,1,0:T(8,128)S(1)} %fusion.7, bf16[8,64,2048]{2,1,0:T(8,128)(2,1)} %all-to-all-done, bf16[1,2048,1024]{2,1,0:T(8,128)(2,1)S(1)} %copy-done.11), kind=kOutput, calls=%fused_computation.22 | convolution fusion | flops 2150629376 | bytes 9437184 | tf_op jit(solution)/shard_map/scd,df->scf/dot_general | solution.py:133
  100.2 12.3 %all-reduce = f32[32]{0:T(128)S(1)} all-reduce(f32[32]{0:T(128)S(1)} %exponential_dynamic-update-slice_fusion), channel_id=2, replica_groups=mesh['ep'=8,'tp'=4] {'ep'}, use_global_device_ids=true, to_apply=%add | all-reduce | flops 32 | bytes 256
  113.9 12.3 %while.30 = (s32[]{:T(128)}, f32[4,128,128]{2,1,0:T(8,128)S(1)}, s32[]{:T(128)}, f32[8,4]{1,0:T(8,128)}, f32[8,4,128,128]{3,2,1,0:T(8,128)}) while((s32[]{:T(128)}, f32[4,128,128]{2,1,0:T(8,128)S(1)}, s32[]{:T(128)}, f32[8,4]{1,0:T(8,128)}, f32[8,4,128,128]{3,2,1,0:T(8,128)}) %tuple.79), condition=%wide.region_6.7_spmd.clone.clone, body=%wide.region_5.6_spmd.clone.sunk.clone | while | flops 262148 | bytes 786569 | solution.py:20
  126.2 2.5 %fusion.18 = f32[2,128,4,128]{1,3,2,0:T(8,128)} fusion(f32[2,4,128,128]{3,2,1,0:T(8,128)} %get-tuple-element.124, f32[2,128,4]{1,2,0:T(4,128)S(1)} %copy.82, f32[4,128,128]{2,1,0:T(8,128)S(1)} %get-tuple-element.126, f32[2,4]{1,0:T(2,128)S(1)} %subtract_exponential_fusion.1, bf16[2,128,4,64]{3,1,2,0:T(8,128)(2,1)S(1)} %copy.69, ...), kind=kOutput, calls=%fused_computation.28 | convolution fusion | flops 202244096 | bytes 1576992 | tf_op jit(solution)/shard_map/nihd,nhde->nihe/dot_general | solution.py:88
  128.8 2.6 %multiply_reduce_fusion.1 = (f32[2,128,4]{1,2,0:T(4,128)S(1)}, f32[2,128,4,128]{1,3,2,0:T(8,128)}) fusion(f32[2,128,4,128]{1,3,2,0:T(8,128)} %fusion.18, bf16[2,128,4,128]{3,2,1,0:T(4,128)(2,1)S(1)} %copy-done.4, bf16[2,128,4,128]{3,1,2,0:T(8,128)(2,1)S(1)} %copy-done.3, f32[2,4,128]{2,1,0:T(4,128)S(1)} %copy.75, ...), kind=kOutput, calls=%fused_computation.41 | convolution fusion | flops 68680704 | bytes 1859584 | tf_op jit(solution)/shard_map/nhij,njhd->nihd/dot_general | solution.py:69
  133.1 1.8 fusion.34
  135.0 18.3 %all-gather.8.cloned.1.call-done = bf16[8,64,4096]{2,1,0:T(8,128)(2,1)} async-done(((bf16[8,64,1024]{2,1,0:T(8,128)(2,1)}), bf16[8,64,4096]{2,1,0:T(8,128)(2,1)}) %all-gather.8.cloned.1.call-update) | async-done | bytes 4194320 | tf_op jit(solution)/shard_map/all_gather | solution.py:137
  153.3 6.6 %fusion.14 = bf16[8,64,512]{2,1,0:T(8,128)(2,1)} fusion(bf16[8,64,4096]{2,1,0:T(8,128)(2,1)} %all-gather.8.cloned.1.call-done, bf16[1,4096,512]{2,1,0:T(8,128)(2,1)} %param.29), kind=kOutput, calls=%fused_computation.23 | convolution fusion | flops 2147745792 | bytes 8912896 | tf_op jit(solution)/shard_map/scf,fd->scd/dot_general | solution.py:135
  159.9 5.6 %all-to-all-start.1 = ((bf16[8,64,512]{2,1,0:T(8,128)(2,1)}), bf16[8,64,512]{2,1,0:T(8,128)(2,1)S(1)}, u32[]{:S(2)}, u32[]{:S(2)}) async-start(bf16[8,64,512]{2,1,0:T(8,128)(2,1)} %fusion.14), calls=%async_computation.1 | async-start | bytes 1048576 | tf_op jit(solution)/shard_map/all_to_all | solution.py:141
  165.7 16.5 %all-gather.6.cloned.1.call-done = bf16[256,2048]{1,0:T(8,128)(2,1)} async-done(((bf16[256,512]{1,0:T(8,128)(2,1)}), bf16[256,2048]{1,0:T(8,128)(2,1)}) %all-gather.6.cloned.1.call-update) | async-done | bytes 1048592 | tf_op jit(solution)/shard_map/all_gather | solution.py:101
  182.1 2.6 %convolution_convert_fusion = bf16[256,512]{1,0:T(8,128)(2,1)} fusion(bf16[256,2048]{1,0:T(8,128)(2,1)} %all-gather.6.cloned.1.call-done, bf16[2048,512]{1,0:T(8,128)(2,1)S(1)} %copy-done), kind=kOutput, calls=%fused_computation.29 | convolution fusion | flops 537001984 | bytes 3407872 | tf_op jit(solution)/shard_map/dot_general | solution.py:100
  184.8 2.6 %gather_fusion.1 = bf16[512,512]{1,0:T(8,128)(2,1)} fusion(bf16[512,512]{1,0:T(8,128)(2,1)S(1)} %bitcast.99, s32[1024]{0:T(1024)S(1)} %pad_clamp_fusion), kind=kCustom, calls=%fused_computation.1 | custom fusion | bytes 1050624 | tf_op jit(solution)/shard_map/gather | solution.py:142
  187.4 1.7 reshape.227
  189.1 2.1 %multiply_reduce_fusion = bf16[256,512]{1,0:T(8,128)(2,1)} fusion(f32[256,2,512]{2,1,0:T(2,128)S(1)} %reshape.227, f32[256,2]{1,0:T(8,128)S(1)} %copy.88), kind=kLoop, calls=%fused_computation.31 | loop fusion | flops 393216 | bytes 1312768 | tf_op jit(solution)/shard_map/reduce_sum | solution.py:143
  (110 shorter events, 34.1 us)
Async XLA Ops:
  7.2 175.0 %copy-start = (bf16[2048,512]{1,0:T(8,128)(2,1)S(1)}, bf16[2048,512]{1,0:T(8,128)(2,1)}, u32[]{:S(2)}) copy-start(bf16[2048,512]{1,0:T(8,128)(2,1)} %param.22) | copy-start | bytes 6291460
  20.5 5.7 %copy-start.8 = (bf16[256,512]{1,0:T(8,128)(2,1)S(1)}, bf16[256,512]{1,0:T(8,128)(2,1)}, u32[]{:S(2)}) copy-start(bf16[256,512]{1,0:T(8,128)(2,1)} %param.17) | copy-start | bytes 786436
  20.5 67.7 %all-to-all-start = ((bf16[8,64,2048]{2,1,0:T(8,128)(2,1)}), bf16[8,64,2048]{2,1,0:T(8,128)(2,1)}, u32[]{:S(2)}, u32[]{:S(2)}) async-start(bf16[8,64,2048]{2,1,0:T(8,128)(2,1)} %bitcast.100), calls=%async_computation | async-start | bytes 4194304 | tf_op jit(solution)/shard_map/all_to_all | solution.py:131
  26.1 87.8 %all-gather.10.cloned.1.call-start = ((), (), s32[]{:S(2)}) async-start(), calls=%async_computation.4 | async-start | bytes 2359296 | tf_op jit(solution)/shard_map/all_gather | solution.py:11
  27.7 5.2 %copy-start.9 = (f32[256,4]{0,1:T(4,128)S(1)}, f32[256,4]{0,1:T(4,128)}, u32[]{:S(2)}) copy-start(f32[256,4]{0,1:T(4,128)} %param.21) | copy-start | bytes 12292
  38.5 0.7 copy-start.2
  42.6 0.7 copy-start.1
  43.3 110.0 %all-gather.8.cloned.1.call-start = ((), (), s32[]{:S(2)}) async-start(), calls=%async_computation.3 | async-start | bytes 5242880 | tf_op jit(solution)/shard_map/all_gather | solution.py:137
  88.1 5.3 %copy-start.11 = (bf16[1,2048,1024]{2,1,0:T(8,128)(2,1)S(1)}, bf16[1,2048,1024]{2,1,0:T(8,128)(2,1)}, u32[]{:S(2)}) copy-start(bf16[1,2048,1024]{2,1,0:T(8,128)(2,1)} %param.28) | copy-start | bytes 12582916
  93.4 5.4 %copy-start.12 = (u32[32]{0:T(128)S(1)}, u32[32]{0:T(128)}, u32[]{:S(2)}) copy-start(u32[32]{0:T(128)} %constant.105) | copy-start | bytes 388
  93.4 19.7 %copy-start.7 = (bf16[256,4,64]{0,2,1:T(8,128)(2,1)S(1)}, bf16[256,4,64]{0,2,1:T(8,128)(2,1)}, u32[]{:S(2)}) copy-start(bf16[256,4,64]{0,2,1:T(8,128)(2,1)} %get-tuple-element.183) | copy-start | bytes 393220
  93.5 20.0 %copy-start.6 = (bf16[256,4,64]{0,2,1:T(8,128)(2,1)S(1)}, bf16[256,4,64]{0,2,1:T(8,128)(2,1)}, u32[]{:S(2)}) copy-start(bf16[256,4,64]{0,2,1:T(8,128)(2,1)} %get-tuple-element.184) | copy-start | bytes 393220
  98.7 15.0 %copy-start.5 = (f32[2,128,4]{2,1,0:T(8,128)S(1)}, f32[2,128,4]{2,1,0:T(8,128)}, u32[]{:S(2)}) copy-start(f32[2,128,4]{2,1,0:T(8,128)} %get-tuple-element.191) | copy-start | bytes 12292
  98.7 83.5 %all-gather.6.cloned.1.call-start = ((), (), s32[]{:S(2)}) async-start(), calls=%async_computation.2 | async-start | bytes 1310720 | tf_op jit(solution)/shard_map/all_gather | solution.py:101
  113.9 14.9 %copy-start.3 = (bf16[2,128,4,128]{3,1,2,0:T(8,128)(2,1)S(1)}, bf16[2,128,4,128]{3,1,2,0:T(8,128)(2,1)}, u32[]{:S(2)}) copy-start(bf16[2,128,4,128]{3,1,2,0:T(8,128)(2,1)} %copy-done.2) | copy-start | bytes 786436
  113.9 14.9 %copy-start.4 = (bf16[2,128,4,128]{3,2,1,0:T(4,128)(2,1)S(1)}, bf16[2,128,4,128]{3,2,1,0:T(4,128)(2,1)}, u32[]{:S(2)}) copy-start(bf16[2,128,4,128]{3,2,1,0:T(4,128)(2,1)} %reshape.218) | copy-start | bytes 786436
  135.0 30.5 %copy-start.10 = (f32[256,2]{0,1:T(2,128)S(1)}, f32[256,2]{0,1:T(2,128)}, u32[]{:S(2)}) copy-start(f32[256,2]{0,1:T(2,128)} %param.26) | copy-start | bytes 6148
  159.9 24.8 %all-to-all-start.1 = ((bf16[8,64,512]{2,1,0:T(8,128)(2,1)}), bf16[8,64,512]{2,1,0:T(8,128)(2,1)S(1)}, u32[]{:S(2)}, u32[]{:S(2)}) async-start(bf16[8,64,512]{2,1,0:T(8,128)(2,1)} %fusion.14), calls=%async_computation.1 | async-start | bytes 1048576 | tf_op jit(solution)/shard_map/all_to_all | solution.py:141
Sparse Core Ops, SparseCore 0:
  43.4 44.0 all-gather.9
  98.8 54.4 all-gather.7
  155.7 26.3 all-gather.5
where the time goes:
time: 201 us; the launch traced here: 198 us
  waiting for transfers between devices  79.7 us (40%)
  local copies, waits for them, and re-layouts  30.9 us (15%)
  matrix products  26.5 us (13%)
  other arithmetic  22 us (11%)
  between operations  14.8 us (7%)
  blocking collectives  12.3 us (6%)
  starting transfers between devices  11.3 us (6%)
    all_to_all x1, waiting for transfers between devices, expert_half(): lax.all_to_all(outgoing, 'ep', split_axis=0, concat_axis=0, tiled=True)  44.8 us
    all_gather x1, waiting for transfers between devices, expert_half(): lax.all_gather(hidden, 'tp', axis=2, tiled=True)  18.3 us
    all_gather x1, waiting for transfers between devices, retention_half(): lax.all_gather(head_out, 'tp', axis=1, tiled=True)  16.5 us
    unnamed x1, blocking collectives  12.3 us
    select_n x7, other arithmetic, turn(): jnp.where(position < mine, new, old)  7.34 us
    dot_general x1, matrix products, expert_half(): jnp.einsum('scf,fd->scd', lax.all_gather(hidden, 'tp', axis=2, tiled=True...  6.6 us
    all_to_all x1, starting transfers between devices, expert_half(): lax.all_to_all(outgoing, 'ep', split_axis=0, concat_axis=0, tiled=True)  5.62 us
    all_to_all x1, starting transfers between devices, expert_half(): lax.all_to_all(expert_out, 'ep', split_axis=0, concat_axis=0, tiled=True)  5.56 us
  transfers between devices with their start and end apart: 5, of which 3 were waited for; matrix products, arithmetic and copies ran while one was open for 30% of the time, Pallas kernels for 0%

commit v1 on v0

v1 whole, which is shorter than its diff:
```python
import functools

import jax
import jax.numpy as jnp
from jax import lax
from jax.experimental import pallas as pl
from jax.experimental.pallas import tpu as pltpu
from jax.sharding import PartitionSpec as P

BLOCK = 128
CHUNKS = 2
MESH = pl.DeviceIdType.MESH
F32 = jnp.float32
BF16 = jnp.bfloat16


def each(low, high, body):
    if high - low <= 8:
        for index in range(low, high):
            body(index)
    else:

        @pl.loop(low, high)
        def _(index):
            body(index)


def span(index, size):
    return pl.ds(pl.multiple_of(index * size, size), size)


def split(value):
    high = value.astype(BF16)
    return high, (value - high.astype(F32)).astype(BF16)


def dot(a, b, dims=((1,), (0,))):
    return lax.dot_general(a, b, (dims, ((), ())), preferred_element_type=F32)


class Gather:
    def __init__(self, tp, region, half, send, recv):
        self.tp, self.region, self.half, self.send, self.recv = tp, region, half, send, recv
        self.me = lax.axis_index("tp")

    def copy(self, ref, slot, to):
        return pltpu.make_async_remote_copy(
            src_ref=ref, dst_ref=ref, send_sem=self.send(slot), recv_sem=self.recv(slot),
            device_id={"tp": to}, device_id_type=MESH,
        )

    def outs(self):
        me, tp = self.me, self.tp
        if tp == 4:
            return [self.copy(self.region(me), k - 1, me ^ k) for k in (1, 2)]
        return [self.copy(self.region(me), k - 1, lax.rem(me + k, tp)) for k in range(1, tp)]

    def hops(self):
        me = self.me
        return [
            self.copy(self.half(me ^ 1, 0), 2, me ^ 2),
            self.copy(self.half(me ^ 2, 1), 3, me ^ 1),
        ]

    def start(self):
        for copy in self.outs():
            copy.start()

    def forward(self):
        if self.tp == 4:
            me = self.me
            hops = self.hops()
            for k in (1, 2):
                self.copy(self.region(me ^ k), k - 1, me ^ k).wait_recv()
                hops[k - 1].start()

    def finish(self):
        me, tp = self.me, self.tp
        if tp == 4:
            self.copy(self.half(me ^ 3, 0), 2, me ^ 2).wait_recv()
            self.copy(self.half(me ^ 3, 1), 3, me ^ 1).wait_recv()
        else:
            for k in range(1, tp):
                owner = lax.rem(me + tp - k, tp)
                self.copy(self.region(owner), k - 1, owner).wait_recv()

    def drain(self):
        for copy in self.outs() + (self.hops() if self.tp == 4 else []):
            copy.wait_send()


def kernel(
    ep, tp,
    q_ref, k_ref, v_ref, g_ref, ld_ref, cos_ref, sin_ref, rows_ref, gain_ref, routes_ref, rw_ref,
    wo_hbm, wg_hbm, wu_hbm, wd_hbm,
    mix_ref, moe_ref,
    wo, wg, wu, wd, normed, p0, p1, og, partner_rows, x, h, eo, ret, ho, state, landed, excl,
    rq, inside, cums,
    w_sem, z_send, z_recv, f_send, f_recv, h_send, h_recv, r_send, r_recv, m_send, m_recv,
    s_send, s_recv,
):
    e, t = lax.axis_index("ep"), lax.axis_index("tp")
    rows, d = rows_ref.shape
    cap = 2 * rows // ep
    dq = d // tp
    ff = wd.shape[0]
    fq = ff // tp
    heads = ld_ref.shape[1]
    hd = q_ref.shape[1] // heads
    blocks = rows // BLOCK
    chunk = ep * cap // CHUNKS
    half_ep = ep // CHUNKS
    pieces = 2 if fq >= 512 else 1
    piece = fq // pieces

    barrier = pltpu.get_barrier_semaphore()

    def greet_ep(off):
        pl.semaphore_signal(barrier, inc=1, device_id={"ep": e ^ off}, device_id_type=MESH)

    each(1, ep, greet_ep)
    for k in range(1, tp):
        pl.semaphore_signal(
            barrier, inc=1, device_id={"tp": lax.rem(t + k, tp)}, device_id_type=MESH
        )

    loads = [
        pltpu.make_async_copy(src, dst, w_sem.at[i])
        for i, (src, dst) in enumerate(
            ((wg_hbm.at[0], wg), (wu_hbm.at[0], wu), (wd_hbm.at[0], wd), (wo_hbm, wo))
        )
    ]
    for load in loads:
        load.start()

    step_rows = 32

    @pl.loop(0, rows // step_rows)
    def _(i):
        at = span(i, step_rows)
        val = rows_ref[at, :].astype(F32)
        scale = lax.rsqrt(jnp.mean(val * val, axis=-1, keepdims=True) + 1e-06)
        normed[at, :] = (val * scale * gain_ref[...].astype(F32)).astype(BF16)

    lanes = lax.broadcasted_iota(jnp.int32, (rows, 128), 1)
    hot = [(routes_ref[:, k : k + 1] == lanes).astype(F32) for k in range(2)]
    before = (
        lax.broadcasted_iota(jnp.int32, (rows, rows), 0)
        > lax.broadcasted_iota(jnp.int32, (rows, rows), 1)
    ).astype(F32).astype(BF16)
    rank = dot(before, (hot[0] + hot[1]).astype(BF16))
    slots = lax.broadcasted_iota(jnp.int32, (rows, ep * cap), 1)
    small = lax.broadcasted_iota(jnp.int32, (rows, cap), 1)
    targets = []
    for k, ref in ((0, p0), (1, p1)):
        target = routes_ref[:, k : k + 1] * cap + jnp.sum(
            rank * hot[k], axis=1, keepdims=True
        ).astype(jnp.int32)
        targets.append(target)
        ref[...] = (slots == target).astype(F32).astype(BF16)
    both = p0[...] + p1[...]
    og[...] = dot(both, normed[:, span(t, dq)], ((0,), (0,))).astype(BF16)

    def block_of(dest):
        base = small + dest * cap
        return ((base == targets[0]) | (base == targets[1])).astype(F32).astype(BF16)

    partner_rows[...] = dot(block_of(e ^ 1), normed[...], ((0,), (0,))).astype(BF16)
    x[span(e, cap), :] = dot(block_of(e), normed[...], ((0,), (0,))).astype(BF16)

    pl.semaphore_wait(barrier, ep - 1 + tp - 1)

    def z_copy(off, here):
        other = e ^ off
        if isinstance(off, int) and off == 1:
            src, dst = partner_rows, x.at[span(other if here else e, cap), :]
        else:
            src = og.at[span(other, cap), :]
            dst = x.at[span(other if here else e, cap), span(t, dq)]
        return pltpu.make_async_remote_copy(
            src_ref=src, dst_ref=dst, send_sem=z_send.at[other],
            recv_sem=z_recv.at[other if here else e],
            device_id={"ep": other}, device_id_type=MESH,
        )

    z_copy(1, False).start()
    each(2, ep, lambda off: z_copy(off, False).start())

    row_i = lax.broadcasted_iota(jnp.int32, (BLOCK, BLOCK), 0)
    col_j = lax.broadcasted_iota(jnp.int32, (BLOCK, BLOCK), 1)
    causal = row_i >= col_j
    lower = causal.astype(F32)
    factor = hd ** (-0.5)
    for b in range(blocks):
        at = slice(b * BLOCK, (b + 1) * BLOCK)
        cums[at, :] = lax.dot_general(
            lower, ld_ref[at, :], (((1,), (0,)), ((), ())),
            preferred_element_type=F32, precision=lax.Precision.HIGHEST,
        )
    decay_at = heads * hd
    for n in range(heads):
        cols = slice(n * hd, (n + 1) * hd)
        total = None
        gone = None
        for b in range(blocks):
            at = slice(b * BLOCK, (b + 1) * BLOCK)
            cos, sin = cos_ref[at, :], sin_ref[at, :]

            def turned(ref):
                val = ref[at, cols].astype(F32)
                return val * cos + pltpu.roll(val, hd // 2, 1) * sin

            qb = turned(q_ref).astype(BF16)
            kb = (turned(k_ref) * factor).astype(BF16)
            vb = v_ref[at, cols]
            rq[at, cols] = qb
            cum = jnp.broadcast_to(cums[at, n : n + 1], (BLOCK, BLOCK))
            spread = cum - cum.T
            weight = jnp.where(causal, jnp.exp(jnp.where(causal, spread, 0.0)), 0.0)
            scores = dot(qb, kb, ((1,), (1,)))
            inside[at, cols] = dot((scores * weight).astype(BF16), vb)
            ending = cum[BLOCK - 1 : BLOCK, :]
            k_hi, k_lo = split(kb.astype(F32) * jnp.exp(ending - cum))
            update = dot(k_hi, vb, ((0,), (0,))) + dot(k_lo, vb, ((0,), (0,)))
            if b == 0:
                total, gone = update, ending
            else:
                if b < blocks:
                    pass
                total = jnp.exp(ending) * total + update
                gone = gone + ending
            if b < blocks - 1:
                excl[1 + b, n * hd : (n + 1) * hd, :] = total
        state[0, n * hd : (n + 1) * hd, :] = total
        state[0, decay_at + n : decay_at + n + 1, :] = jnp.exp(gone)

    excl[0, :decay_at, :] = jnp.zeros((decay_at, hd), F32)
    excl[0, decay_at : decay_at + heads, :] = jnp.ones((heads, hd), F32)

    rounds = state.shape[0]

    def s_copy(r):
        return pltpu.make_async_remote_copy(
            src_ref=state.at[r], dst_ref=landed.at[r], send_sem=s_send.at[r],
            recv_sem=s_recv.at[r], device_id={"ep": lax.rem(e + 2**r, ep)}, device_id_type=MESH,
        )

    def scan_send(r):
        @pl.when(e + 2**r < ep)
        def _():
            s_copy(r).start()

    def scan_take(r):
        last = r == rounds - 1

        @pl.when(e >= 2**r)
        def _():
            s_copy(r).wait_recv()
            for n in range(heads):
                at = slice(n * hd, (n + 1) * hd)
                da = slice(decay_at + n, decay_at + n + 1)
                came, came_d = landed[r, at, :], landed[r, da, :]
                own_d = excl[0, da, :]
                excl[0, at, :] = own_d * came + excl[0, at, :]
                excl[0, da, :] = own_d * came_d
                if not last:
                    mine_d = state[r, da, :]
                    state[r + 1, at, :] = mine_d * came + state[r, at, :]
                    state[r + 1, da, :] = mine_d * came_d

        if not last:

            @pl.when(e < 2**r)
            def _():
                state[r + 1, : decay_at + heads, :] = state[r, : decay_at + heads, :]

    def row_gather(off):
        other = e ^ off
        start = other * cap

        def half(owner, k):
            return x.at[
                pl.ds(pl.multiple_of(start + k * (cap // 2), cap // 2), cap // 2), span(owner, dq)
            ]

        return Gather(
            tp, lambda owner: x.at[span(other, cap), span(owner, dq)], half,
            lambda slot: f_send.at[other, slot], lambda slot: f_recv.at[other, slot],
        )

    def part_of(c):
        return (e // half_ep) ^ c

    def hid_gather(c, j):
        base = part_of(c) * chunk

        def cols(owner):
            return pl.ds(pl.multiple_of(owner * fq + j * piece, piece), piece)

        return Gather(
            tp,
            lambda owner: h.at[pl.ds(pl.multiple_of(base, chunk), chunk), cols(owner)],
            lambda owner, k: h.at[
                pl.ds(pl.multiple_of(base + k * (chunk // 2), chunk // 2), chunk // 2), cols(owner)
            ],
            lambda slot: h_send.at[c * pieces + j, slot],
            lambda slot: h_recv.at[c * pieces + j, slot],
        )

    mix_gather = Gather(
        tp, lambda owner: ho.at[:, span(owner, heads * hd)],
        lambda owner, k: ho.at[k * (rows // 2) : (k + 1) * (rows // 2), span(owner, heads * hd)],
        lambda slot: m_send.at[slot], lambda slot: m_recv.at[slot],
    )

    def take_rows(off):
        z_copy(off, True).wait_recv()
        row_gather(off).start()

    def hidden_piece(c, j):
        at = pl.ds(pl.multiple_of(part_of(c) * chunk, chunk), chunk)
        tile = min(256, piece)

        @pl.loop(0, piece // tile)
        def _(i):
            cols = pl.ds(pl.multiple_of(j * piece + i * tile, tile), tile)
            held = x[at, :]
            gate = dot(held, wg[:, cols])
            up = dot(held, wu[:, cols])
            hid = (gate / (1.0 + jnp.exp(-gate)) * up).astype(BF16)
            h[at, pl.ds(pl.multiple_of(t * fq + j * piece + i * tile, tile), tile)] = hid

        hid_gather(c, j).start()

    def back_copy(off, here):
        other = e ^ off
        return pltpu.make_async_remote_copy(
            src_ref=eo.at[span(other, cap), :], dst_ref=ret.at[span(other if here else e, cap), :],
            send_sem=r_send.at[other], recv_sem=r_recv.at[other if here else e],
            device_id={"ep": other}, device_id_type=MESH,
        )

    def down(c):
        at = pl.ds(pl.multiple_of(part_of(c) * chunk, chunk), chunk)
        tile = min(256, dq)

        @pl.loop(0, dq // tile)
        def _(i):
            cols = pl.ds(pl.multiple_of(i * tile, tile), tile)
            eo[at, cols] = dot(h[at, :], wd[:, cols]).astype(BF16)

        if c == 0:
            ret[span(e, cap), :] = eo[span(e, cap), :]
        each(max(1, c * half_ep), (c + 1) * half_ep, lambda off: back_copy(off, False).start())

    scan_send(0)
    each(2, half_ep, take_rows)
    each(half_ep, ep, take_rows)
    scan_take(0)
    if rounds > 1:
        scan_send(1)
    each(2, half_ep, lambda off: row_gather(off).forward())
    loads[0].wait()
    loads[1].wait()
    z_copy(1, True).wait_recv()
    each(2, half_ep, lambda off: row_gather(off).finish())
    hidden_piece(0, 0)
    each(half_ep, ep, lambda off: row_gather(off).forward())
    for j in range(1, pieces):
        hidden_piece(0, j)
    if rounds > 1:
        scan_take(1)
    if rounds > 2:
        scan_send(2)
    each(half_ep, ep, lambda off: row_gather(off).finish())
    hid_gather(0, 0).forward()
    hidden_piece(1, 0)
    for j in range(1, pieces):
        hid_gather(0, j).forward()
    for j in range(1, pieces):
        hidden_piece(1, j)
    for r in range(2, rounds):
        scan_take(r)
        if r + 1 < rounds:
            scan_send(r + 1)

    for n in range(heads):
        cols = slice(n * hd, (n + 1) * hd)
        sat = slice(n * hd, (n + 1) * hd)
        entering = excl[0, sat, :]
        gone = None
        for b in range(blocks):
            at = slice(b * BLOCK, (b + 1) * BLOCK)
            cum = jnp.broadcast_to(cums[at, n : n + 1], (BLOCK, hd))
            held = entering if b == 0 else jnp.exp(gone) * entering + excl[b, sat, :]
            hi, lo = split(held)
            qb = rq[at, cols]
            retained = inside[at, cols] + (dot(qb, hi) + dot(qb, lo)) * jnp.exp(cum)
            scale = lax.rsqrt(jnp.mean(retained * retained, axis=-1, keepdims=True) + 1e-05)
            gate = g_ref[at, cols].astype(F32)
            out = (retained * scale * (gate / (1.0 + jnp.exp(-gate)))).astype(BF16)
            ho[at, pl.ds(pl.multiple_of(t * heads * hd + n * hd, hd), hd)] = out
            ending = cum[BLOCK - 1 : BLOCK, :]
            gone = ending if gone is None else gone + ending
    mix_gather.start()

    loads[2].wait()
    loads[3].wait()
    for j in range(pieces):
        hid_gather(0, j).finish()
    hid_gather(1, 0).forward()
    down(0)
    for j in range(1, pieces):
        hid_gather(1, j).forward()
    mix_gather.forward()
    for j in range(pieces):
        hid_gather(1, j).finish()
    down(1)
    mix_gather.finish()
    tile = min(256, dq)

    @pl.loop(0, dq // tile)
    def _(i):
        cols = pl.ds(pl.multiple_of(i * tile, tile), tile)
        mix_ref[:, cols] = dot(ho[...], wo[:, cols]).astype(BF16)

    each(1, ep, lambda off: back_copy(off, True).wait_recv())

    @pl.loop(0, dq // tile)
    def _(i):
        cols = pl.ds(pl.multiple_of(i * tile, tile), tile)
        came = ret[:, cols]
        moe_ref[:, cols] = (
            dot(p0[...], came) * rw_ref[:, 0:1] + dot(p1[...], came) * rw_ref[:, 1:2]
        ).astype(BF16)

    z_copy(1, False).wait_send()
    each(2, ep, lambda off: z_copy(off, False).wait_send())
    each(2, ep, lambda off: row_gather(off).drain())
    each(1, ep, lambda off: back_copy(off, False).wait_send())
    for c in range(CHUNKS):
        for j in range(pieces):
            hid_gather(c, j).drain()
    mix_gather.drain()
    for r in range(rounds):

        @pl.when(e + 2**r < ep)
        def _():
            s_copy(r).wait_send()


def on_device(
    ep, tp,
    queries, keys, values, gates, log_decay, out_weight, moe_rows, moe_gain, routes,
    route_weights, gate_proj, up_proj, down_proj,
):
    rows, d = moe_rows.shape
    heads = log_decay.shape[1]
    width = queries.shape[1]
    hd = width // heads
    cap = 2 * rows // ep
    dq = d // tp
    fq = gate_proj.shape[2]
    ff = down_proj.shape[1]
    rounds = (ep - 1).bit_length()
    slots = max(4, tp - 1)
    pieces = CHUNKS * 2
    blocks = rows // BLOCK
    positions = (lax.axis_index("ep") * rows + jnp.arange(rows, dtype=jnp.int32)).astype(F32)
    half = hd // 2
    inverse = 10000.0 ** (-jnp.arange(half, dtype=F32) / half)
    angles = positions[:, None] * jnp.tile(inverse, 2)[None, :]
    sign = jnp.where(jnp.arange(hd) < half, -1.0, 1.0).astype(F32)
    cos, sin = jnp.cos(angles), jnp.sin(angles) * sign[None, :]
    srows = heads * hd + 8 * ((heads + 7) // 8)
    vmem = pl.BlockSpec(memory_space=pltpu.VMEM)
    hbm = pl.BlockSpec(memory_space=pl.ANY)
    dma = pltpu.SemaphoreType.DMA
    out = jax.ShapeDtypeStruct((rows, dq), BF16)
    return pl.pallas_call(
        functools.partial(kernel, ep, tp),
        out_shape=(out, out),
        in_specs=[vmem] * 11 + [hbm] * 4,
        out_specs=(vmem, vmem),
        scratch_shapes=[
            pltpu.VMEM(out_weight.shape, BF16),
            pltpu.VMEM((d, fq), BF16),
            pltpu.VMEM((d, fq), BF16),
            pltpu.VMEM((ff, dq), BF16),
            pltpu.VMEM((rows, d), BF16),
            pltpu.VMEM((rows, ep * cap), BF16),
            pltpu.VMEM((rows, ep * cap), BF16),
            pltpu.VMEM((ep * cap, dq), BF16),
            pltpu.VMEM((cap, d), BF16),
            pltpu.VMEM((ep * cap, d), BF16),
            pltpu.VMEM((ep * cap, ff), BF16),
            pltpu.VMEM((ep * cap, dq), BF16),
            pltpu.VMEM((ep * cap, dq), BF16),
            pltpu.VMEM((rows, width * tp), BF16),
            pltpu.VMEM((rounds, srows, hd), F32),
            pltpu.VMEM((rounds, srows, hd), F32),
            pltpu.VMEM((blocks, srows, hd), F32),
            pltpu.VMEM((rows, width), BF16),
            pltpu.VMEM((rows, width), F32),
            pltpu.VMEM((rows, heads), F32),
            dma((4,)),
            dma((ep,)), dma((ep,)),
            dma((ep, slots)), dma((ep, slots)),
            dma((pieces, slots)), dma((pieces, slots)),
            dma((ep,)), dma((ep,)),
            dma((slots,)), dma((slots,)),
            dma((rounds,)), dma((rounds,)),
        ],
        compiler_params=pltpu.CompilerParams(
            collective_id=0, has_side_effects=True, vmem_limit_bytes=60 * 1024 * 1024
        ),
    )(
        queries, keys, values, gates, log_decay, cos, sin, moe_rows, moe_gain[None, :], routes,
        route_weights, out_weight, gate_proj, up_proj, down_proj,
    )


def solution(mesh):
    placed = (
        P("ep", "tp"), P("ep", "tp"), P("ep", "tp"), P("ep", "tp"), P("ep", "tp"),
        P(None, "tp"), P("ep", None), P(), P("ep", None), P("ep", None),
        P("ep", None, "tp"), P("ep", None, "tp"), P("ep", None, "tp"),
    )
    return jax.shard_map(
        functools.partial(on_device, mesh.shape["ep"], mesh.shape["tp"]),
        mesh=mesh, in_specs=placed, out_specs=(P("ep", "tp"), P("ep", "tp")), check_vma=False,
    )
```

time: 201 us -> 96.3 us (0.48); the launches traced: 198 us -> 95.9 us
  Pallas kernels: 0 us -> 84.9 us
  waiting for transfers between devices: 79.7 us -> 0 us
  matrix products: 26.5 us -> 0 us
  local copies, waits for them, and re-layouts: 30.9 us -> 9.12 us
  other arithmetic: 22 us -> 1.26 us
  between operations: 14.8 us -> 0.66 us
  blocking collectives: 12.3 us -> 0 us
  starting transfers between devices: 11.3 us -> 0 us
    pallas_call x0 -> x1, Pallas kernels: none -> 84.9 us  [on_device(): pl.pallas_call(functools.partial(kernel, ep, tp), out_shape=(out, out), i...]
    all_to_all x2 -> x0, waiting for transfers between devices: 44.8 us -> none  [the longest x1 44.8 us: expert_half(): lax.all_to_all(outgoing, 'ep', split_axis=0, concat_axis=0, tiled=True)]
    all_gather x3 -> x0, waiting for transfers between devices: 34.9 us -> none  [the longest x1 18.3 us: expert_half(): lax.all_gather(hidden, 'tp', axis=2, tiled=True)]
    dot_general x7 -> x0, matrix products: 26.5 us -> none  [the longest x1 6.6 us: expert_half(): jnp.einsum('scf,fd->scd', lax.all_gather(hidden, 'tp', axis=2, tiled=True...]
    unnamed x1 -> x0, blocking collectives: 12.3 us -> none
    all_to_all x2 -> x0, starting transfers between devices: 11.2 us -> none  [the longest x1 5.62 us: expert_half(): lax.all_to_all(outgoing, 'ep', split_axis=0, concat_axis=0, tiled=True)]
    select_n x10 -> x1, other arithmetic: 7.36 us -> 0.01 us  [on_device(): sign = jnp.where(jnp.arange(hd) < half, -1.0, 1.0).astype(F32)]
    gather x2 -> x0, local copies, waits for them, and re-layouts: 5.91 us -> none  [the longest x1 3.29 us: expert_half(): outgoing = normed[source_row].reshape(experts, capacity, feat_width)]
  transfers between devices with their start and end apart: 5 -> 0, of which waited for: 3 -> 0; matrix products, arithmetic and copies ran while one was open for 30% -> 0% of each run, Pallas kernels for 0% -> 0%
where the time goes in v1:
time: 96.3 us; the launch traced here: 95.9 us
  Pallas kernels  84.9 us (88%)
  local copies, waits for them, and re-layouts  9.12 us (9%)
  other arithmetic  1.26 us (1%)
    pallas_call x1, Pallas kernels, on_device(): pl.pallas_call(functools.partial(kernel, ep, tp), out_shape=(out, out), i...  84.9 us
    unnamed x5, local copies, waits for them, and re-layouts  7.75 us

profile of v1, /device:TPU:17, one launch (start us, length us, event | category | flops | bytes accessed | tf_op | source)
XLA Modules:
  0.0 95.9 jit_solution(7741880761195967067)
XLA Ops:
  0.7 0.1 mul.28
  0.8 1.3 %broadcast_in_dim.15.gain_ref = bf16[1,2048]{1,0:T(2,128)(2,1)} reshape(bf16[2048]{0:T(1024)(128)(2,1)} %param.20) | data formatting | bytes 8192 | tf_op jit(solution)/shard_map/broadcast_in_dim | solution.py:518
  2.0 1.5 %copy.15.ld_ref = f32[256,4]{1,0:T(8,128)} copy(f32[256,4]{0,1:T(4,128)} %param.17) | data formatting | bytes 8192 | tf_op args[4]
  3.5 1.5 %copy.16.routes_ref = s32[256,2]{1,0:T(8,128)} copy(s32[256,2]{0,1:T(2,128)} %param.21) | data formatting | bytes 4096 | tf_op args[8]
  5.0 1.5 %copy.17.rw_ref = f32[256,2]{1,0:T(8,128)} copy(f32[256,2]{0,1:T(2,128)} %param.22) | data formatting | bytes 4096 | tf_op args[9]
  6.5 1.2 %fusion = (f32[256,128]{1,0:T(8,128)}, f32[256,128]{1,0:T(8,128)}) fusion(f32[128]{0:T(128)S(1)} %compare_select_fusion, f32[128]{0:T(128)S(1)} %mul.28, f32[256]{0:T(256)S(1)} %add_convert_fusion), kind=kLoop, calls=%fused_computation.2 | loop fusion | flops 65536 | bytes 264192 | tf_op jit(solution)/shard_map/mul | solution.py:474
  7.7 84.9 %shard_map.140 = (bf16[256,512]{1,0:T(8,128)(2,1)}, bf16[256,512]{1,0:T(8,128)(2,1)}) custom-call(bf16[256,512]{1,0:T(8,128)(2,1)} %q_ref.1, bf16[256,512]{1,0:T(8,128)(2,1)} %k_ref.1, bf16[256,512]{1,0:T(8,128)(2,1)} %v_ref.1, bf16[256,512]{1,0:T(8,128)(2,1)} %g_ref.1, f32[256,4]{1,0:T(8,128)} %copy.15.ld_ref, f32[256,128]{1,0:T(8,128)} %get-tuple-element.3.cos_ref, ...), custom_call_target="tpu_custom_call" | custom-call | tf_op jit(solution)/shard_map/pallas_call | solution.py:480
  92.6 1.7 %copy.20 = bf16[256,512]{1,0:T(8,128)(2,1)} copy(bf16[256,512]{1,0:T(8,128)(2,1)} %get-tuple-element.6) | data formatting | bytes 524288
  94.3 1.7 %copy.21 = bf16[256,512]{1,0:T(8,128)(2,1)} copy(bf16[256,512]{1,0:T(8,128)(2,1)} %get-tuple-element.7) | data formatting | bytes 524288
  (4 shorter events, 0.0 us)

commit v2 on v1

--- a/solution.py
+++ b/solution.py
@@ -95,7 +95,7 @@
     wo_hbm, wg_hbm, wu_hbm, wd_hbm,
     mix_ref, moe_ref,
     wo, wg, wu, wd, normed, p0, p1, og, partner_rows, x, h, eo, ret, ho, state, landed, excl,
-    rq, inside, cums,
+    rq, inside, cums, pack, narrow,
     w_sem, z_send, z_recv, f_send, f_recv, h_send, h_recv, r_send, r_recv, m_send, m_recv,
     s_send, s_recv,
 ):
@@ -105,7 +105,7 @@
     dq = d // tp
     ff = wd.shape[0]
     fq = ff // tp
-    heads = ld_ref.shape[1]
+    heads = ld_ref.shape[0]
     hd = q_ref.shape[1] // heads
     blocks = rows // BLOCK
     chunk = ep * cap // CHUNKS
@@ -133,6 +133,14 @@
     for load in loads:
         load.start()
 
+    pack[...] = jnp.zeros_like(pack)
+    pack[0:2, :] = routes_ref[...].astype(F32)
+    pack[2:4, :] = rw_ref[...]
+    pack[4 : 4 + heads, :] = ld_ref[...]
+    for b in range(rows // 128):
+        narrow[b * 128 : (b + 1) * 128, :] = pack[:, b * 128 : (b + 1) * 128].T
+    routes = [narrow[:, k : k + 1].astype(jnp.int32) for k in range(2)]
+
     step_rows = 32
 
     @pl.loop(0, rows // step_rows)
@@ -140,10 +148,14 @@
         at = span(i, step_rows)
         val = rows_ref[at, :].astype(F32)
         scale = lax.rsqrt(jnp.mean(val * val, axis=-1, keepdims=True) + 1e-06)
-        normed[at, :] = (val * scale * gain_ref[...].astype(F32)).astype(BF16)
+        for c in range(d // 128):
+            cols = slice(c * 128, (c + 1) * 128)
+            normed[at, cols] = (val[:, cols] * scale * gain_ref[c : c + 1, :].astype(F32)).astype(
+                BF16
+            )
 
     lanes = lax.broadcasted_iota(jnp.int32, (rows, 128), 1)
-    hot = [(routes_ref[:, k : k + 1] == lanes).astype(F32) for k in range(2)]
+    hot = [(routes[k] == lanes).astype(F32) for k in range(2)]
     before = (
         lax.broadcasted_iota(jnp.int32, (rows, rows), 0)
         > lax.broadcasted_iota(jnp.int32, (rows, rows), 1)
@@ -153,7 +165,7 @@
     small = lax.broadcasted_iota(jnp.int32, (rows, cap), 1)
     targets = []
     for k, ref in ((0, p0), (1, p1)):
-        target = routes_ref[:, k : k + 1] * cap + jnp.sum(
+        target = routes[k] * cap + jnp.sum(
             rank * hot[k], axis=1, keepdims=True
         ).astype(jnp.int32)
         targets.append(target)
@@ -194,7 +206,7 @@
     for b in range(blocks):
         at = slice(b * BLOCK, (b + 1) * BLOCK)
         cums[at, :] = lax.dot_general(
-            lower, ld_ref[at, :], (((1,), (0,)), ((), ())),
+            lower, narrow[at, :], (((1,), (0,)), ((), ())),
             preferred_element_type=F32, precision=lax.Precision.HIGHEST,
         )
     decay_at = heads * hd
@@ -214,7 +226,7 @@
             kb = (turned(k_ref) * factor).astype(BF16)
             vb = v_ref[at, cols]
             rq[at, cols] = qb
-            cum = jnp.broadcast_to(cums[at, n : n + 1], (BLOCK, BLOCK))
+            cum = jnp.broadcast_to(cums[at, 4 + n : 5 + n], (BLOCK, BLOCK))
             spread = cum - cum.T
             weight = jnp.where(causal, jnp.exp(jnp.where(causal, spread, 0.0)), 0.0)
             scores = dot(qb, kb, ((1,), (1,)))
@@ -391,7 +403,7 @@
         gone = None
         for b in range(blocks):
             at = slice(b * BLOCK, (b + 1) * BLOCK)
-            cum = jnp.broadcast_to(cums[at, n : n + 1], (BLOCK, hd))
+            cum = jnp.broadcast_to(cums[at, 4 + n : 5 + n], (BLOCK, hd))
             held = entering if b == 0 else jnp.exp(gone) * entering + excl[b, sat, :]
             hi, lo = split(held)
             qb = rq[at, cols]
@@ -431,7 +443,7 @@
         cols = pl.ds(pl.multiple_of(i * tile, tile), tile)
         came = ret[:, cols]
         moe_ref[:, cols] = (
-            dot(p0[...], came) * rw_ref[:, 0:1] + dot(p1[...], came) * rw_ref[:, 1:2]
+            dot(p0[...], came) * narrow[:, 2:3] + dot(p1[...], came) * narrow[:, 3:4]
         ).astype(BF16)
 
     z_copy(1, False).wait_send()
@@ -502,7 +514,9 @@
             pltpu.VMEM((blocks, srows, hd), F32),
             pltpu.VMEM((rows, width), BF16),
             pltpu.VMEM((rows, width), F32),
-            pltpu.VMEM((rows, heads), F32),
+            pltpu.VMEM((rows, 128), F32),
+            pltpu.VMEM((128, rows), F32),
+            pltpu.VMEM((rows, 128), F32),
             dma((4,)),
             dma((ep,)), dma((ep,)),
             dma((ep, slots)), dma((ep, slots)),
@@ -515,8 +529,8 @@
             collective_id=0, has_side_effects=True, vmem_limit_bytes=60 * 1024 * 1024
         ),
     )(
-        queries, keys, values, gates, log_decay, cos, sin, moe_rows, moe_gain[None, :], routes,
-        route_weights, out_weight, gate_proj, up_proj, down_proj,
+        queries, keys, values, gates, log_decay.T, cos, sin, moe_rows, moe_gain.reshape(-1, 128),
+        routes.T, route_weights.T, out_weight, gate_proj, up_proj, down_proj,
     )
 
 

time: 96.3 us -> 90.3 us (0.938)
  local copies, waits for them, and re-layouts: 9.12 us -> 3.42 us
    unnamed x5 -> x2, local copies, waits for them, and re-layouts: 7.75 us -> 3.34 us
    broadcast_in_dim x1 -> x0, local copies, waits for them, and re-layouts: 1.29 us -> none  [on_device(): moe_gain[None, :]]
where the time goes in v2:
time: 90.3 us; the launch traced here: 90.1 us
  Pallas kernels  84.8 us (94%)
  local copies, waits for them, and re-layouts  3.42 us (4%)
  other arithmetic  1.26 us (1%)
    pallas_call x1, Pallas kernels, on_device(): pl.pallas_call(functools.partial(kernel, ep, tp), out_shape=(out, out), i...  84.8 us
    unnamed x2, local copies, waits for them, and re-layouts  3.34 us

profile of v2, /device:TPU:17, one launch (start us, length us, event | category | flops | bytes accessed | tf_op | source)
XLA Modules:
  0.0 90.1 jit_solution(14856713039399539993)
XLA Ops:
  0.7 0.1 mul.28
  0.8 1.2 %fusion = (f32[256,128]{1,0:T(8,128)}, f32[256,128]{1,0:T(8,128)}) fusion(f32[128]{0:T(128)S(1)} %compare_select_fusion, f32[128]{0:T(128)S(1)} %mul.28, f32[256]{0:T(256)S(1)} %add_convert_fusion), kind=kLoop, calls=%fused_computation.2 | loop fusion | flops 65536 | bytes 264192 | tf_op jit(solution)/shard_map/mul | solution.py:486
  2.0 84.8 %shard_map.140 = (bf16[256,512]{1,0:T(8,128)(2,1)}, bf16[256,512]{1,0:T(8,128)(2,1)}) custom-call(bf16[256,512]{1,0:T(8,128)(2,1)} %q_ref.1, bf16[256,512]{1,0:T(8,128)(2,1)} %k_ref.1, bf16[256,512]{1,0:T(8,128)(2,1)} %v_ref.1, bf16[256,512]{1,0:T(8,128)(2,1)} %g_ref.1, f32[4,256]{1,0:T(4,128)} %bitcast.4, f32[256,128]{1,0:T(8,128)} %get-tuple-element.3.cos_ref, ...), custom_call_target="tpu_custom_call" | custom-call | tf_op jit(solution)/shard_map/pallas_call | solution.py:492
  86.8 1.7 %copy.17 = bf16[256,512]{1,0:T(8,128)(2,1)} copy(bf16[256,512]{1,0:T(8,128)(2,1)} %get-tuple-element.6) | data formatting | bytes 524288
  88.5 1.7 %copy.18 = bf16[256,512]{1,0:T(8,128)(2,1)} copy(bf16[256,512]{1,0:T(8,128)(2,1)} %get-tuple-element.7) | data formatting | bytes 524288
  (4 shorter events, 0.0 us)
